TPU v7x, 256 devices: a whole 4x4x8 slice. The times are simulated.
256 devices in a mesh: sp: 32 (over z, y), tp: 8 (over x, core).
Axes of the slice: x: 4, y: 4, z: 8, core: 2. Of those that a mesh axis runs over, the one named last changes fastest.
Arguments:
- queries: bfloat16 [9216, 2048], P('sp', 'tp'), as said below
- key_vectors: bfloat16 [9216, 2048], P('sp', 'tp'), as said below
- latents: bfloat16 [9216, 2048], P('sp'), as said below
- value_weight: bfloat16 [2048, 2048], P(None, 'tp'), as said below
- log_sums: float32 [9216, 32], P('sp', 'tp'), as said below
- out_first: bfloat16 [9216, 2048], P('sp', 'tp'), as said below
- out_second: bfloat16 [9216, 2048], P('sp', 'tp'), as said below
- cotangent: bfloat16 [9216, 2048], P('sp', 'tp'), may hold values from -6 to 6
- head_lambda: float32 [16], P('tp'), may hold values from 0.3 to 0.8
Outputs:
- grad_queries: float32 [9216, 2048], P('sp', 'tp')
- grad_keys: float32 [9216, 2048], P('sp', 'tp')
- grad_latents: bfloat16 [9216, 2048], P('sp', 'tp')
- grad_weight: float32 [2048, 2048], P('sp', 'tp')
Inputs may be any that keep to these rules, and one draw needn't show every extreme that they name: queries with entries of standard deviation 1.75. `key_vectors`: keys with entries of standard deviation 1. `latents`: inputs of standard deviation 1. `value_weight`: weights scaled by the inverse square root of 2048. `log_sums`: each row's log-sum of exponentials of its causal scores, for the given queries and keys. `out_first`: the first map's attention output for the given queries, keys, values and log-sums. `out_second`: the second map's attention output, likewise.
All inputs are finite; a program needn't handle non-finite values.
Results may differ from a plain program's by a relative error of at most 0.022.
Values may be sent and summed in bfloat16 or wider, within the bound.
A program may use at most 192 MiB of HBM per device.

v0:
```python
import jax
import jax.numpy as jnp
from jax import lax
from jax.sharding import PartitionSpec as P

DH = 64
DV = 128


def side_by_side(arrays, axis, dim, along):
    widths = [a.shape[along] for a in arrays]
    both = jnp.concatenate(arrays, axis=along)
    out = lax.all_gather(both, axis, axis=dim, tiled=True)
    return tuple(jnp.split(out, [sum(widths[:k]) for k in range(1, len(widths))], axis=along))


def cut_along(x, dim, devices):
    before, after = (x.shape[:dim], x.shape[dim + 1 :])
    return jnp.moveaxis(x.reshape(*before, devices, -1, *after), dim, 0)


def summed_on_arrival(x, axis, dim):
    parts = cut_along(x, dim, lax.axis_size(axis))
    arrived = lax.all_to_all(parts, axis, split_axis=0, concat_axis=0, tiled=True)
    return arrived.astype(jnp.float32).sum(axis=0)


def row_terms(out_first, out_second, cotangent, head_lambda):
    count = out_first.shape[0]
    head_count = head_lambda.shape[0]
    first = out_first.astype(jnp.float32).reshape(count, head_count, DV)
    second = out_second.astype(jnp.float32).reshape(count, head_count, DV)
    mixed = first - head_lambda[None, :, None] * second
    inverse = lax.rsqrt(jnp.mean(mixed * mixed, axis=-1, keepdims=True) + 1e-06)
    normed = mixed * inverse
    grad_out = cotangent.astype(jnp.float32).reshape(count, head_count, DV)
    grad_mixed = inverse * (grad_out - normed * jnp.mean(grad_out * normed, axis=-1, keepdims=True))
    grad_rows = grad_mixed.astype(jnp.bfloat16)
    widened = lax.optimization_barrier(grad_rows).astype(jnp.float32)
    row_dots = jnp.stack(
        [jnp.sum(widened * first, axis=-1), jnp.sum(widened * second, axis=-1)], axis=-1
    )
    return (grad_rows.reshape(count, head_count * DV), row_dots.reshape(count, head_count * 2))


def block_grads(
    query_rows, grad_rows, lse_rows, dot_rows, query_pos, key_rows, value_rows, key_pos, head_lambda
):
    count = query_rows.shape[0]
    width = key_rows.shape[0]
    head_count = head_lambda.shape[0]
    score_scale = DH ** (-0.5)
    query_heads = query_rows.reshape(count, head_count, 2, DH)
    key_heads = key_rows.reshape(width, head_count, 2, DH)
    grad_heads = grad_rows.reshape(count, head_count, DV)
    value_heads = value_rows.reshape(width, head_count, DV)
    scores = (
        jnp.einsum("nhad,mhad->hanm", query_heads, key_heads, preferred_element_type=jnp.float32)
        * score_scale
    )
    causal = query_pos[:, None] >= key_pos[None, :]
    shifts = lse_rows.reshape(count, head_count, 2).transpose(1, 2, 0)[..., None]
    probs = jnp.exp(jnp.where(causal, scores - shifts, -1e30))
    d_attn = jnp.einsum("nhe,mhe->hnm", grad_heads, value_heads, preferred_element_type=jnp.float32)
    dots = dot_rows.reshape(count, head_count, 2).transpose(1, 2, 0)[..., None]
    map_weight = jnp.stack([jnp.ones_like(head_lambda), -head_lambda], axis=1)[:, :, None, None]
    d_scores = (map_weight * probs * (d_attn[:, None] - dots)).astype(jnp.bfloat16)
    weights = (probs[:, 0] - head_lambda[:, None, None] * probs[:, 1]).astype(jnp.bfloat16)
    grad_q = (
        jnp.einsum("hanm,mhad->nhad", d_scores, key_heads, preferred_element_type=jnp.float32)
        * score_scale
    )
    grad_k = (
        jnp.einsum("hanm,nhad->mhad", d_scores, query_heads, preferred_element_type=jnp.float32)
        * score_scale
    )
    grad_v = jnp.einsum("hnm,nhe->mhe", weights, grad_heads, preferred_element_type=jnp.float32)
    return (grad_q.reshape(count, -1), grad_k.reshape(width, -1), grad_v.reshape(width, -1))


def per_device(
    queries,
    key_vectors,
    latents,
    value_weight,
    log_sums,
    out_first,
    out_second,
    cotangent,
    head_lambda,
):
    local_rows = queries.shape[0]
    offset = lax.axis_index("sp") * local_rows
    positions = offset + jnp.arange(local_rows, dtype=jnp.int32)
    last_row = offset + local_rows - 1
    values = jnp.dot(latents, value_weight, preferred_element_type=jnp.float32).astype(jnp.bfloat16)
    grad_rows, row_dots = row_terms(out_first, out_second, cotangent, head_lambda)
    gathered_stats = side_by_side((log_sums, row_dots), "sp", 0, 1)
    key_rows, value_rows = side_by_side((key_vectors, values), "sp", 0, 1)
    count = key_rows.shape[0]

    def compute(current):
        key_pos = jnp.arange(count, dtype=jnp.int32)
        grad_q, unused_k, unused_v = block_grads(
            queries,
            grad_rows,
            log_sums,
            row_dots,
            positions,
            key_rows,
            value_rows,
            key_pos,
            head_lambda,
        )
        return grad_q

    grad_queries = lax.cond(
        jnp.int32(0) <= last_row,
        compute,
        lambda current: current,
        jnp.zeros((local_rows, queries.shape[1]), jnp.float32),
    )
    start_totals = (
        jnp.zeros((local_rows, key_vectors.shape[1]), jnp.float32),
        jnp.zeros((local_rows, values.shape[1]), jnp.float32),
    )
    query_rows, grad_piece = side_by_side((queries, grad_rows), "sp", 0, 1)
    add_count = query_rows.shape[0]

    def compute(current):
        query_pos = jnp.arange(add_count, dtype=jnp.int32)
        lse_rows = gathered_stats[0]
        dot_rows = gathered_stats[1]
        unused_q, grad_k, grad_v = block_grads(
            query_rows,
            grad_piece,
            lse_rows,
            dot_rows,
            query_pos,
            key_vectors,
            values,
            positions,
            head_lambda,
        )
        return (grad_k, grad_v)

    grad_keys, grad_values = lax.cond(
        jnp.int32(0) + add_count - 1 >= offset, compute, lambda current: current, start_totals
    )
    values_grad = grad_values.astype(jnp.bfloat16)
    grad_weight = summed_on_arrival(
        lax.dot_general(
            latents, values_grad, (((0,), (0,)), ((), ())), preferred_element_type=jnp.float32
        ).astype(jnp.bfloat16),
        "sp",
        0,
    )
    latent_partial = lax.dot_general(
        values_grad, value_weight, (((1,), (1,)), ((), ())), preferred_element_type=jnp.float32
    )
    grad_latents = lax.psum_scatter(
        latent_partial.astype(jnp.bfloat16), "tp", scatter_dimension=1, tiled=True
    )
    return (grad_queries, grad_keys, grad_latents, grad_weight)


def solution(mesh):
    return jax.shard_map(
        per_device,
        mesh=mesh,
        in_specs=(
            P("sp", "tp"),
            P("sp", "tp"),
            P("sp", None),
            P(None, "tp"),
            P("sp", "tp"),
            P("sp", "tp"),
            P("sp", "tp"),
            P("sp", "tp"),
            P("tp"),
        ),
        out_specs=(P("sp", "tp"), P("sp", "tp"), P("sp", "tp"), P("sp", "tp")),
        check_vma=False,
    )
```

profile of v0, /device:TPU:8, one launch (start us, length us, event | category | flops | bytes accessed | tf_op | source)
XLA Modules:
  0.0 307.0 jit_solution(7757270281936150602)
XLA Ops:
  7.3 0.8 broadcast_bitcast_fusion
  8.1 1.0 convert_bitcast_fusion.1
  9.1 0.9 multiply_reduce_fusion
  10.0 0.1 copy.152
  10.2 1.2 fusion.32
  11.4 0.1 copy.153
  11.5 0.4 mul.122.clone
  11.9 0.4 mul.119.clone
  12.3 1.2 fusion.27
  13.4 1.6 pad_maximum_fusion.1
  15.2 1.7 convolution_convert_fusion.2
  16.9 1.6 pad_maximum_fusion
  18.6 1.1 fusion.31
  19.7 0.3 fusion.28
  20.0 0.1 copy.151
  20.3 0.2 copy.150
  20.6 52.6 %all-gather = f32[32,288,8]{1,2,0:T(8,128)S(1)} all-gather(f32[1,288,8]{1,2,0:T(8,128)S(1)} %maximum_bitcast_fusion), channel_id=1, replica_groups=mesh['sp'=32,'tp'=8] {'sp'}, dimensions={0}, use_global_device_ids=true | all-gather | bytes 304128 | tf_op jit(solution)/shard_map/all_gather | solution.py:13
  73.3 0.2 reshape.96
  73.5 46.7 %all-gather.6.cloned.1.call-done = bf16[9216,512]{1,0:T(8,128)(2,1)} async-done(((bf16[288,512]{1,0:T(8,128)(2,1)}), bf16[9216,512]{1,0:T(8,128)(2,1)}) %all-gather.6.cloned.1.call-update) | async-done | bytes 9437200 | tf_op jit(solution)/shard_map/all_gather | solution.py:13
  120.2 97.8 %conditional.3 = (bf16[288,256]{1,0:T(8,128)(2,1)S(1)}, f32[288,256]{1,0:T(8,128)S(1)}) conditional(s32[]{:T(128)} %convert_element_type.67, () %tuple.26, (f32[2]{0:T(128)S(1)}, s32[288]{0:T(512)S(1)}, bf16[9216,512]{1,0:T(8,128)(2,1)}, bf16[288,256]{1,0:T(8,128)(2,1)S(1)}, f32[9216,8]{0,1:T(8,128)S(1)}, ...), branch_computations={%region_6.7_spmd, %region_7.8_spmd} | conditional | flops 5528862720 | bytes 235193568 | solution.py:147
  120.2 12.9 %copy.135 = bf16[9216,512]{0,1:T(8,128)(2,1)} copy(bf16[9216,512]{1,0:T(8,128)(2,1)} %get-tuple-element.144) | data formatting | bytes 18874368 | tf_op jit(solution)/shard_map
  133.1 8.2 %fusion.35 = (bf16[9216,256]{0,1:T(8,128)(2,1)}, bf16[9216,256]{0,1:T(8,128)(2,1)}) fusion(bf16[9216,512]{0,1:T(8,128)(2,1)} %copy.135), kind=kLoop, calls=%fused_computation.62 | loop fusion | bytes 18874368 | tf_op jit(solution)/shard_map/split | solution.py:14
  141.3 0.1 reshape.80
  141.5 2.9 iota_compare_fusion.1
  144.4 0.2 copy.136
  144.6 21.1 %select_exponential_fusion = f32[2,2,9216,288]{2,3,1,0:T(8,128)} fusion(f32[2,2,9216]{2,1,0:T(2,128)S(1)} %bitcast.141, pred[9216,288]{0,1:T(8,128)(4,1)} %iota_compare_fusion.1, bf16[9216,2,2,64]{0,3,2,1:T(8,128)(2,1)} %bitcast.128, bf16[288,2,2,64]{0,3,2,1:T(8,128)(2,1)S(1)} %bitcast.140), kind=kOutput, calls=%fused_computation.10 | convolution fusion | flops 1390804992 | bytes 50135040 | tf_op jit(solution)/shard_map/cond/branch_1_fun/nhad,mhad->hanm/dot_general | solution.py:58
  165.6 16.9 %fusion.17 = bf16[2,36,8,128]{3,2,1,0:T(8,128)(2,1)S(1)} fusion(bf16[9216,2,128]{0,2,1:T(8,128)(2,1)} %bitcast.126, f32[2,2,9216,288]{2,3,1,0:T(8,128)} %select_exponential_fusion, f32[2]{0:T(128)S(1)} %get-tuple-element.46), kind=kOutput, calls=%fused_computation.21 | convolution fusion | flops 1374953472 | bytes 47333384 | tf_op jit(solution)/shard_map/cond/branch_1_fun/hnm,nhe->mhe/dot_general | solution.py:77
  182.6 0.1 reshape.83
  182.7 11.2 %fusion.20 = f32[2,9216,288]{1,2,0:T(8,128)} fusion(bf16[9216,2,128]{0,2,1:T(8,128)(2,1)} %bitcast.127, bf16[288,256]{1,0:T(8,128)(2,1)S(1)} %get-tuple-element.51), kind=kOutput, calls=%fused_computation.23 | convolution fusion | flops 1358954496 | bytes 26099712 | tf_op jit(solution)/shard_map/cond/branch_1_fun/nhe,mhe->hnm/dot_general | solution.py:64
  193.9 0.1 copy.149
  194.1 23.8 %fusion.13 = f32[2,2,288,64]{2,3,1,0:T(8,128)S(1)} fusion(bf16[9216,2,2,64]{0,3,2,1:T(8,128)(2,1)} %bitcast.129, f32[2,2,9216,288]{2,3,1,0:T(8,128)} %select_exponential_fusion, f32[2,2,9216]{2,1,0:T(2,128)S(1)} %bitcast.132, f32[2,9216,288]{1,2,0:T(8,128)} %fusion.20, f32[2,2]{1,0:T(2,128)S(1)} %stack.17.clone), kind=kOutput, calls=%fused_computation.19 | convolution fusion | flops 1401495552 | bytes 68861968 | tf_op jit(solution)/shard_map/cond/branch_1_fun/hanm,nhad->mhad/dot_general | solution.py:74
  217.9 0.1 copy.146
  218.1 2.9 convolution_convert_fusion
  221.0 0.7 fusion.23
  221.7 1.3 copy.137
  223.0 7.3 %all-to-all-start = ((bf16[32,64,256]{2,1,0:T(8,128)(2,1)}), bf16[32,64,256]{2,1,0:T(8,128)(2,1)S(1)}, u32[]{:S(2)}, u32[]{:S(2)}) async-start(bf16[32,64,256]{2,1,0:T(8,128)(2,1)} %bitcast.24), calls=%async_computation.1 | async-start | bytes 2097152 | tf_op jit(solution)/shard_map/all_to_all | solution.py:24
  230.4 68.7 %conditional.2 = (f32[288,256]{1,0:T(8,128)S(1)}) conditional(s32[]{:T(128)} %convert_element_type.60, () %tuple.24, (f32[2]{0:T(128)S(1)}, s32[288]{0:T(512)S(1)}, bf16[288,256]{1,0:T(8,128)(2,1)S(1)}, bf16[9216,512]{1,0:T(8,128)(2,1)}, f32[288,4]{0,1:T(4,128)S(1)}, /*index=5*/bf16[9216,512]{1,0:T(8,128)(2,1)}, bf16[288,2,128]{2,0,1:T(8,128)(2,1)S(1)}, ...), branch_computations={%region_4.0_spmd, %region_5.6_spmd} | conditional | flops 4153909248 | bytes 120048872 | solution.py:117
  230.4 12.7 %copy.130 = bf16[9216,512]{0,1:T(8,128)(2,1)} copy(bf16[9216,512]{1,0:T(8,128)(2,1)} %get-tuple-element.139) | data formatting | bytes 18874368 | tf_op jit(solution)/shard_map
  243.1 4.8 %split.26 = bf16[9216,256]{0,1:T(8,128)(2,1)} slice(bf16[9216,512]{0,1:T(8,128)(2,1)} %copy.130), slice={[0:9216], [0:256]} | slice | bytes 9437184 | tf_op jit(solution)/shard_map/split | solution.py:14
  247.9 12.7 %copy.131 = bf16[9216,512]{0,1:T(8,128)(2,1)} copy(bf16[9216,512]{1,0:T(8,128)(2,1)} %get-tuple-element.139) | data formatting | bytes 18874368 | tf_op jit(solution)/shard_map
  260.6 2.3 slice-done
  263.0 8.6 %fusion.37 = f32[2,288,9216]{2,1,0:T(8,128)} fusion(bf16[288,2,128]{2,0,1:T(8,128)(2,1)S(1)} %get-tuple-element.43, bf16[9216,2,128]{0,2,1:T(8,128)(2,1)S(1)} %bitcast.125), kind=kOutput, calls=%fused_computation.64 | convolution fusion | flops 1358954496 | bytes 26099712 | tf_op jit(solution)/shard_map/cond/branch_1_fun/nhe,mhe->hnm/dot_general | solution.py:64
  271.8 2.9 iota_compare_fusion
  274.7 0.2 copy.129
  274.9 24.0 %fusion.4 = f32[2,2,288,64]{2,3,1,0:T(8,128)S(1)} fusion(bf16[9216,2,2,64]{0,3,2,1:T(8,128)(2,1)} %bitcast.130, f32[2,2,288]{2,1,0:T(2,128)S(1)} %bitcast.142, f32[2,288,9216]{2,1,0:T(8,128)} %fusion.37, f32[2,2,288]{2,1,0:T(2,128)S(1)} %bitcast.143, f32[2,2]{1,0:T(2,128)S(1)} %stack.15.clone, pred[288,9216]{1,0:T(8,128)(4,1)} %iota_compare_fusion, ...), kind=kOutput, calls=%fused_computation.5 | convolution fusion | flops 2792300544 | bytes 29058064 | tf_op jit(solution)/shard_map/cond/branch_1_fun/hanm,mhad->nhad/dot_general | solution.py:70
  298.9 0.1 copy.144
  299.1 0.8 convert_reduce_fusion
  299.9 0.6 copy-done.1
  (42 shorter events, 0.9 us)
Async XLA Ops:
  7.2 8.0 %copy-start = (bf16[288,2048]{1,0:T(8,128)(2,1)S(1)}, bf16[288,2048]{1,0:T(8,128)(2,1)}, u32[]{:S(2)}) copy-start(bf16[288,2048]{1,0:T(8,128)(2,1)} %param.15) | copy-start | bytes 3538948
  7.2 113.0 %copy-start.7 = (f32[2]{0:T(128)S(1)}, f32[2]{0:T(128)}, u32[]{:S(2)}) copy-start(f32[2]{0:T(128)} %param.21) | copy-start | bytes 28
  7.2 113.0 %copy-start.2 = (bf16[288,256]{1,0:T(8,128)(2,1)S(1)}, bf16[288,256]{1,0:T(8,128)(2,1)}, u32[]{:S(2)}) copy-start(bf16[288,256]{1,0:T(8,128)(2,1)} %param.14) | copy-start | bytes 442372
  7.2 13.4 %copy-start.6 = (f32[288,4]{0,1:T(4,128)S(1)}, f32[288,4]{0,1:T(4,128)}, u32[]{:S(2)}) copy-start(f32[288,4]{0,1:T(4,128)} %param.17) | copy-start | bytes 13828
  7.2 113.0 %all-gather.6.cloned.1.call-start = ((), (), s32[]{:S(2)}) async-start(), calls=%async_computation.3 | async-start | bytes 9732096 | tf_op jit(solution)/shard_map/all_gather | solution.py:13
  15.1 215.2 %all-gather.4.cloned.1.call-start = ((), (), s32[]{:S(2)}) async-start(), calls=%async_computation.2 | async-start | bytes 9732096 | tf_op jit(solution)/shard_map/all_gather | solution.py:13
  18.5 281.4 %reduce-scatter.2.cloned.1.call-start = ((), (), s32[]{:S(2)}) async-start(), calls=%async_computation.4 | async-start | bytes 1327104 | tf_op jit(solution)/shard_map/reduce_scatter | solution.py:161
  120.2 110.1 %copy-start.3 = (bf16[288,256]{1,0:T(8,128)(2,1)S(1)}, bf16[288,256]{1,0:T(8,128)(2,1)}, u32[]{:S(2)}) copy-start(bf16[288,256]{1,0:T(8,128)(2,1)} %param.13) | copy-start | bytes 442372
  218.1 12.3 %copy-start.4 = (f32[288,256]{1,0:T(8,128)}, f32[288,256]{1,0:T(8,128)S(1)}, u32[]{:S(2)}) copy-start(f32[288,256]{1,0:T(8,128)S(1)} %get-tuple-element.153) | copy-start | bytes 884740
  223.0 76.1 %all-to-all-start = ((bf16[32,64,256]{2,1,0:T(8,128)(2,1)}), bf16[32,64,256]{2,1,0:T(8,128)(2,1)S(1)}, u32[]{:S(2)}, u32[]{:S(2)}) async-start(bf16[32,64,256]{2,1,0:T(8,128)(2,1)} %bitcast.24), calls=%async_computation.1 | async-start | bytes 2097152 | tf_op jit(solution)/shard_map/all_to_all | solution.py:24
  260.6 2.3 slice-start
  299.1 0.8 copy-start.5
  299.1 1.4 copy-start.1
Sparse Core Ops, SparseCore 0:
  15.2 104.9 all-gather.5
  123.4 100.2 all-gather.3
  226.8 33.7 reduce-scatter.1
where the time goes:
time: 308 us; the launch traced here: 307 us
  matrix products  111 us (36%)
  local copies, waits for them, and re-layouts  59.5 us (19%)
  blocking collectives  52.6 us (17%)
  waiting for transfers between devices  46.8 us (15%)
  other arithmetic  15.7 us (5%)
  between operations  14 us (5%)
  starting transfers between devices  7.41 us (2%)
    all_gather x1, blocking collectives, side_by_side(): out = lax.all_gather(both, axis, axis=dim, tiled=True)  52.6 us
    all_gather x2, waiting for transfers between devices, side_by_side(): out = lax.all_gather(both, axis, axis=dim, tiled=True)  46.8 us
    another operation x5, local copies, waits for them, and re-layouts  38.6 us
    dot_general x1, matrix products, block_grads(): jnp.einsum('hanm,mhad->nhad', d_scores, key_heads, preferred_element_type...  24 us
    dot_general x1, matrix products, block_grads(): jnp.einsum('hanm,nhad->mhad', d_scores, query_heads, preferred_element_ty...  23.8 us
    dot_general x1, matrix products, block_grads(): jnp.einsum('nhad,mhad->hanm', query_heads, key_heads, preferred_element_t...  21.1 us
    dot_general x2, matrix products, block_grads(): jnp.einsum('nhe,mhe->hnm', grad_heads, value_heads, preferred_element_typ...  19.9 us
    dot_general x1, matrix products, block_grads(): jnp.einsum('hnm,nhe->mhe', weights, grad_heads, preferred_element_type=jn...  16.9 us
  transfers between devices with their start and end apart: 4, of which 1 were waited for; matrix products, arithmetic and copies ran while one was open for 57% of the time, Pallas kernels for 0%

commit v1 on v0

v1 whole, which is shorter than its diff:
```python
import functools
import math

import jax
import jax.numpy as jnp
from jax import lax
from jax.experimental import pallas as pl
from jax.experimental.pallas import tpu as pltpu
from jax.sharding import PartitionSpec as P

DH = 64
DV = 128
NY = 4
NZ = 8
LOG2E = math.log2(math.e)
BF = jnp.bfloat16
F32 = jnp.float32


def cut_along(x, dim, devices):
    before, after = (x.shape[:dim], x.shape[dim + 1 :])
    return jnp.moveaxis(x.reshape(*before, devices, -1, *after), dim, 0)


def summed_on_arrival(x, axis, dim):
    parts = cut_along(x, dim, lax.axis_size(axis))
    arrived = lax.all_to_all(parts, axis, split_axis=0, concat_axis=0, tiled=True)
    return arrived.astype(jnp.float32).sum(axis=0)


def row_terms(out_first, out_second, cotangent, head_lambda):
    count = out_first.shape[0]
    head_count = head_lambda.shape[0]
    first = out_first.astype(jnp.float32).reshape(count, head_count, DV)
    second = out_second.astype(jnp.float32).reshape(count, head_count, DV)
    mixed = first - head_lambda[None, :, None] * second
    inverse = lax.rsqrt(jnp.mean(mixed * mixed, axis=-1, keepdims=True) + 1e-06)
    normed = mixed * inverse
    grad_out = cotangent.astype(jnp.float32).reshape(count, head_count, DV)
    grad_mixed = inverse * (grad_out - normed * jnp.mean(grad_out * normed, axis=-1, keepdims=True))
    grad_rows = grad_mixed.astype(jnp.bfloat16)
    widened = lax.optimization_barrier(grad_rows).astype(jnp.float32)
    row_dots = jnp.stack(
        [jnp.sum(widened * first, axis=-1), jnp.sum(widened * second, axis=-1)], axis=-1
    )
    return (grad_rows.reshape(count, head_count * DV), row_dots.reshape(count, head_count * 2))


def dot(a, b):
    return jnp.dot(a, b, preferred_element_type=F32)


def low_map(x):
    return lax.broadcasted_iota(jnp.int32, x.shape, 1) < DH


def score_terms(m_a, m_b, na_t, nb_t, shift0, shift1, dot0, dot1, mask):
    low = low_map(m_a)
    none = jnp.zeros_like(m_a)
    s0 = dot(jnp.where(low, m_a, none), na_t) * (LOG2E * DH ** (-0.5)) - shift0
    s1 = dot(jnp.where(low, none, m_a), na_t) * (LOG2E * DH ** (-0.5)) - shift1
    da = dot(m_b, nb_t)
    if mask is not None:
        s0 = jnp.where(mask, s0, -1e30)
        s1 = jnp.where(mask, s1, -1e30)
    p0 = jnp.exp2(s0)
    p1 = jnp.exp2(s1)
    ds0 = (p0 * (da - dot0)).astype(BF)
    ds1 = (p1 * (dot1 - da)).astype(BF)
    weights = (p0 - p1).astype(BF)
    return ds0, ds1, weights


def attention_kernel(
    ma_ref, na_ref, mb_ref, nb_ref, sta_ref, stb_ref,
    gq_ref, gk_ref, gv_ref,
    ma, mb, sta, stb, na, nb, nat, nvt, nbt, ndt,
    acc_a, acc_v, acc_b, own_a, own_b,
    full_a, full_b, send_a, send_b, recv_a, recv_b, nsend_a, nsend_b, nrecv_a, nrecv_b,
    yg_send, yg_recv, ma_send, ma_recv, sta_send, sta_recv, mb_send, mb_recv,
    ra_send, ra_recv, rb_send, rb_recv, na_send, na_recv, nb_send, nb_recv,
):
    rows = ma_ref.shape[0]
    wide = NY * rows
    sp = lax.axis_index("sp")
    z = sp // NY
    y = sp % NY

    def copy(src, dst, ssem, rsem, target):
        return pltpu.make_async_remote_copy(
            src_ref=src, dst_ref=dst, send_sem=ssem, recv_sem=rsem,
            device_id={"sp": target}, device_id_type=pl.DeviceIdType.MESH,
        )

    barrier = pltpu.get_barrier_semaphore()
    y_peers = [z * NY + (y + k) % NY for k in range(1, NY)]
    z_peers = [((z + k) % NZ) * NY + y for k in range(1, NZ)]
    for peer in y_peers + z_peers:
        pl.semaphore_signal(barrier, inc=1, device_id={"sp": peer}, device_id_type=pl.DeviceIdType.MESH)
    pl.semaphore_wait(barrier, len(y_peers) + len(z_peers))

    def span(index):
        return pl.ds(pl.multiple_of(index * rows, rows), rows)

    below = jnp.maximum(sp - NY, 0)
    above = jnp.minimum(sp + NY, NZ * NY - 1)

    def ma_copy(src, c):
        return copy(src, ma.at[c], ma_send.at[c], ma_recv.at[c], below)

    def sta_copy(src, c):
        return copy(src, sta.at[c], sta_send.at[c], sta_recv.at[c], below)

    def mb_copy(src, c):
        return copy(src, mb.at[c], mb_send.at[c], mb_recv.at[c], above)

    def y_copies(k, slot, target):
        return [
            copy(na_ref, na.at[span(slot)], yg_send.at[k, 0], yg_recv.at[slot, 0], target),
            copy(nb_ref, nb.at[span(slot)], yg_send.at[k, 1], yg_recv.at[slot, 1], target),
            copy(stb_ref, stb.at[slot], yg_send.at[k, 2], yg_recv.at[slot, 2], target),
        ]

    for k, peer in enumerate(y_peers):
        for c in y_copies(k, y, peer):
            c.start()

    @pl.when(z > 0)
    def _():
        sta_copy(sta_ref, z).start()
        ma_copy(ma_ref, z).start()

    @pl.when(z < NZ - 1)
    def _():
        mb_copy(mb_ref, z).start()

    na[span(y), :] = na_ref[...]
    nb[span(y), :] = nb_ref[...]
    stb[y] = stb_ref[...]

    for k, peer in enumerate(y_peers):
        for c in y_copies(k, (y + k + 1) % NY, peer):
            c.wait_recv()

    nat[...] = na[:, :DV].T
    nvt[...] = na[:, DV:].T
    nbt[...] = nb[:, :DV].T
    ndt[...] = nb[:, DV:].T
    stb[NY] = stb[0] + stb[1] + stb[2] + stb[3]

    def take_a(t):
        sta_copy(sta.at[z + t], z + t).wait_recv()
        ma_copy(ma.at[z + t], z + t).wait_recv()

    def take_b(t):
        mb_copy(mb.at[z - t], z - t).wait_recv()

    def pass_a(t):
        @pl.when(jnp.logical_and(z > 0, z + t < NZ))
        def _():
            take_a(t)
            sta_copy(sta.at[z + t], z + t).start()
            ma_copy(ma.at[z + t], z + t).start()

    def pass_b(t):
        @pl.when(jnp.logical_and(z < NZ - 1, z - t >= 0))
        def _():
            take_b(t)
            mb_copy(mb.at[z - t], z - t).start()

    def unit_a(m, stats, mask):
        st = stats.T[:rows]
        m_a = m[:, :DV]
        m_b = m[:, DV:]
        ds0, ds1, weights = score_terms(
            m_a, m_b, nat[...], nvt[...], st[:, 0:1], st[:, 1:2], st[:, 2:3], st[:, 3:4], mask
        )
        k_all = na[:, :DV]
        d0 = dot(ds0, k_all)
        d1 = dot(ds1, k_all)
        m_at = m_a.T
        parts = (dot(m_at[:DH], ds0), dot(m_at[DH:], ds1), dot(m_b.T, weights))
        return jnp.where(low_map(d0), d0, d1), parts

    def unit_b(m, mask):
        st = stb[NY]
        m_a = m[:, :DV]
        m_b = m[:, DV:]
        ds0, ds1, weights = score_terms(
            m_a, m_b, nbt[...], ndt[...], st[0:1], st[1:2], st[2:3], st[3:4], mask
        )
        q_all = nb[:, :DV]
        d0 = dot(ds0, q_all)
        d1 = dot(ds1, q_all)
        dv = dot(weights, nb[:, DV:])
        m_at = m_a.T
        parts = (dot(m_at[:DH], ds0), dot(m_at[DH:], ds1))
        return jnp.where(low_map(d0), d0, d1), dv, parts

    lane = lax.broadcasted_iota(jnp.int32, (rows, wide), 1)
    place = lax.broadcasted_iota(jnp.int32, (rows, wide), 0) + y * rows

    pass_a(1)
    pass_b(1)
    moved, parts = unit_a(ma_ref[...], sta_ref[...], place >= lane)
    own_a[...] = moved
    acc_a[:DH] = parts[0]
    acc_a[DH:] = parts[1]
    acc_v[...] = parts[2]
    moved, moved_v, parts = unit_b(mb_ref[...], lane >= place)
    own_b[:, :DV] = moved
    own_b[:, DV:] = moved_v
    acc_b[:DH] = parts[0]
    acc_b[DH:] = parts[1]

    def out_a(t):
        return copy(
            send_a.at[t], recv_a.at[z], ra_send.at[t], ra_recv.at[z], jnp.minimum(sp + t * NY, NZ * NY - 1)
        )

    def out_b(t):
        return copy(
            send_b.at[t], recv_b.at[z], rb_send.at[t], rb_recv.at[z], jnp.maximum(sp - t * NY, 0)
        )

    def step(t, carry):
        pass_a(t + 1)
        pass_b(t + 1)

        @pl.when(z + t < NZ)
        def _():
            @pl.when(z == 0)
            def _():
                take_a(t)

            moved, parts = unit_a(ma[z + t], sta[z + t], None)
            send_a[t] = moved.astype(BF)
            out_a(t).start()
            acc_a[:DH] += parts[0]
            acc_a[DH:] += parts[1]
            acc_v[...] += parts[2]

        @pl.when(z - t >= 0)
        def _():
            @pl.when(z == NZ - 1)
            def _():
                take_b(t)

            moved, moved_v, parts = unit_b(mb[z - t], None)
            send_b[t, :, :DV] = moved.astype(BF)
            send_b[t, :, DV:] = moved_v.astype(BF)
            out_b(t).start()
            acc_b[:DH] += parts[0]
            acc_b[DH:] += parts[1]

        return carry

    lax.fori_loop(1, NZ, step, 0)

    def y_out_a(k, mine, theirs, target):
        return copy(nsend_a.at[span(theirs)], nrecv_a.at[mine], na_send.at[k], na_recv.at[mine], target)

    def y_out_b(k, mine, theirs, target):
        return copy(nsend_b.at[span(theirs)], nrecv_b.at[mine], nb_send.at[k], nb_recv.at[mine], target)

    full_a[:, :DV] = acc_a[...].T
    full_a[:, DV:] = acc_v[...].T
    nsend_a[...] = full_a[...].astype(BF)
    for k, peer in enumerate(y_peers):
        y_out_a(k, y, (y + k + 1) % NY, peer).start()
    full_b[...] = acc_b[...].T
    nsend_b[...] = full_b[...].astype(BF)
    for k, peer in enumerate(y_peers):
        y_out_b(k, y, (y + k + 1) % NY, peer).start()

    def add_a(j, carry):
        copy(send_a.at[0], recv_a.at[j], ra_send.at[0], ra_recv.at[j], below).wait_recv()
        own_a[...] += recv_a[j].astype(F32)
        return carry

    def add_b(j, carry):
        copy(send_b.at[0], recv_b.at[j], rb_send.at[0], rb_recv.at[j], above).wait_recv()
        own_b[...] += recv_b[j].astype(F32)
        return carry

    lax.fori_loop(0, z, add_a, 0)
    lax.fori_loop(z + 1, NZ, add_b, 0)

    total_a = full_a[span(y), :]
    total_b = full_b[span(y), :]
    for k, peer in enumerate(y_peers):
        slot = (y + k + 1) % NY
        y_out_a(k, slot, y, peer).wait_recv()
        total_a += nrecv_a[slot].astype(F32)
    gv_ref[:, :DV] = total_a[:, DV:].astype(BF)
    gv_ref[:, DV:] = own_b[:, DV:].astype(BF)
    scale = DH ** (-0.5)
    gk_ref[:, :DV] = total_a[:, :DV] * scale
    gk_ref[:, DV:] = own_b[:, :DV] * scale
    for k, peer in enumerate(y_peers):
        slot = (y + k + 1) % NY
        y_out_b(k, slot, y, peer).wait_recv()
        total_b += nrecv_b[slot].astype(F32)
    gq_ref[:, :DV] = own_a[...] * scale
    gq_ref[:, DV:] = total_b * scale

    for k, peer in enumerate(y_peers):
        for c in y_copies(k, y, peer):
            c.wait_send()
        y_out_a(k, y, y, peer).wait_send()
        y_out_b(k, y, y, peer).wait_send()

    def drain_a(t, carry):
        @pl.when(t > 0)
        def _():
            out_a(t).wait_send()

        @pl.when(z > 0)
        def _():
            sta_copy(sta.at[z + t], z + t).wait_send()
            ma_copy(ma.at[z + t], z + t).wait_send()

        return carry

    def drain_b(t, carry):
        @pl.when(t > 0)
        def _():
            out_b(t).wait_send()

        @pl.when(z < NZ - 1)
        def _():
            mb_copy(mb.at[z - t], z - t).wait_send()

        return carry

    lax.fori_loop(0, NZ - z, drain_a, 0)
    lax.fori_loop(0, z + 1, drain_b, 0)


def attention(ma, na, mb, nb, sta, stb):
    rows = ma.shape[0]
    wide = NY * rows
    dma = pltpu.SemaphoreType.DMA
    vmem = pltpu.VMEM
    whole = pl.BlockSpec(memory_space=pltpu.VMEM)
    return pl.pallas_call(
        attention_kernel,
        out_shape=(
            jax.ShapeDtypeStruct((rows, 2 * DV), F32),
            jax.ShapeDtypeStruct((rows, 2 * DV), F32),
            jax.ShapeDtypeStruct((rows, 2 * DV), BF),
        ),
        in_specs=[whole] * 6,
        out_specs=(whole,) * 3,
        scratch_shapes=[
            vmem((NZ, rows, 2 * DV), BF),
            vmem((NZ, rows, 2 * DV), BF),
            vmem((NZ,) + sta.shape, F32),
            vmem((NY + 1,) + stb.shape, F32),
            vmem((wide, 2 * DV), BF),
            vmem((wide, 2 * DV), BF),
            vmem((DV, wide), BF),
            vmem((DV, wide), BF),
            vmem((DV, wide), BF),
            vmem((DV, wide), BF),
            vmem((DV, wide), F32),
            vmem((DV, wide), F32),
            vmem((DV, wide), F32),
            vmem((rows, DV), F32),
            vmem((rows, 2 * DV), F32),
            vmem((wide, 2 * DV), F32),
            vmem((wide, DV), F32),
            vmem((NZ, rows, DV), BF),
            vmem((NZ, rows, 2 * DV), BF),
            vmem((NZ, rows, DV), BF),
            vmem((NZ, rows, 2 * DV), BF),
            vmem((wide, 2 * DV), BF),
            vmem((wide, DV), BF),
            vmem((NY, rows, 2 * DV), BF),
            vmem((NY, rows, DV), BF),
            dma((NY - 1, 3)),
            dma((NY, 3)),
        ]
        + [dma((NZ,))] * 10
        + [dma((NY,))] * 4,
        compiler_params=pltpu.CompilerParams(
            collective_id=0, has_side_effects=True, vmem_limit_bytes=60 * 1024 * 1024
        ),
        cost_estimate=pl.CostEstimate(flops=20_000_000_000, bytes_accessed=4_000_000, transcendentals=6_000_000),
    )(ma, na, mb, nb, sta, stb)


def per_device(
    queries,
    key_vectors,
    latents,
    value_weight,
    log_sums,
    out_first,
    out_second,
    cotangent,
    head_lambda,
):
    rows = queries.shape[0]
    values = jnp.dot(latents, value_weight, preferred_element_type=jnp.float32).astype(jnp.bfloat16)
    grad_rows, row_dots = row_terms(out_first, out_second, cotangent, head_lambda)
    shifts = log_sums.reshape(rows, 2, 2) * LOG2E
    shifts = shifts - jnp.stack([jnp.zeros_like(head_lambda), jnp.log2(head_lambda)], axis=1)[None]
    stats = jnp.concatenate([shifts, row_dots.reshape(rows, 2, 2)], axis=2)
    stats = jnp.pad(stats.transpose(1, 2, 0), ((0, 0), (0, 4), (0, 0)))
    sta = jnp.pad(stats[0], ((0, 0), (0, -rows % 128)))
    y = lax.axis_index("sp") % NY
    stb = lax.dynamic_update_slice(
        jnp.zeros((8, NY * rows), F32), stats[1], (jnp.int32(0), (y * rows).astype(jnp.int32))
    )
    ma = jnp.concatenate([queries[:, :DV], grad_rows[:, :DV]], axis=1)
    nb = jnp.concatenate([queries[:, DV:], grad_rows[:, DV:]], axis=1)
    na = jnp.concatenate([key_vectors[:, :DV], values[:, :DV]], axis=1)
    mb = jnp.concatenate([key_vectors[:, DV:], values[:, DV:]], axis=1)
    grad_queries, grad_keys, values_grad = attention(ma, na, mb, nb, sta, stb)
    grad_weight = summed_on_arrival(
        lax.dot_general(
            latents, values_grad, (((0,), (0,)), ((), ())), preferred_element_type=jnp.float32
        ).astype(jnp.bfloat16),
        "sp",
        0,
    )
    latent_partial = lax.dot_general(
        values_grad, value_weight, (((1,), (1,)), ((), ())), preferred_element_type=jnp.float32
    )
    grad_latents = lax.psum_scatter(
        latent_partial.astype(jnp.bfloat16), "tp", scatter_dimension=1, tiled=True
    )
    return (grad_queries, grad_keys, grad_latents, grad_weight)


def solution(mesh):
    return jax.shard_map(
        per_device,
        mesh=mesh,
        in_specs=(
            P("sp", "tp"),
            P("sp", "tp"),
            P("sp", None),
            P(None, "tp"),
            P("sp", "tp"),
            P("sp", "tp"),
            P("sp", "tp"),
            P("sp", "tp"),
            P("tp"),
        ),
        out_specs=(P("sp", "tp"), P("sp", "tp"), P("sp", "tp"), P("sp", "tp")),
        check_vma=False,
    )
```

time: 308 us -> 147 us (0.48)
  matrix products: 111 us -> 4.91 us
  Pallas kernels: 0 us -> 84.3 us
  blocking collectives: 52.6 us -> 0 us
  local copies, waits for them, and re-layouts: 59.5 us -> 7.67 us
  waiting for transfers between devices: 46.8 us -> 22.9 us
  other arithmetic: 15.7 us -> 6.64 us
    dot_general x6 -> x0, matrix products: 106 us -> none  [the longest x1 24 us: block_grads(): jnp.einsum('hanm,mhad->nhad', d_scores, key_heads, preferred_element_type...]
    pallas_call x0 -> x1, Pallas kernels: none -> 84.3 us  [attention(): pl.pallas_call(attention_kernel, out_shape=(jax.ShapeDtypeStruct((rows, 2...]
    all_gather x1 -> x0, blocking collectives: 52.6 us -> none  [side_by_side(): out = lax.all_gather(both, axis, axis=dim, tiled=True)]
    all_gather x2 -> x0, waiting for transfers between devices: 46.8 us -> none  [side_by_side(): out = lax.all_gather(both, axis, axis=dim, tiled=True)]
    another operation x7 -> x1, local copies, waits for them, and re-layouts: 38.8 us -> 0.07 us  [per_device(): jnp.stack([jnp.zeros_like(head_lambda), jnp.log2(head_lambda)], axis=1)]
    all_to_all x1, waiting for transfers between devices: 0.01 us -> 19.3 us  [summed_on_arrival(): lax.all_to_all(parts, axis, split_axis=0, concat_axis=0, tiled=True)]
    split x5 -> x0, local copies, waits for them, and re-layouts: 15.4 us -> none  [side_by_side(): jnp.split(out, [sum(widths[:k]) for k in range(1, len(widths))], axis=along)]
    ge x2 -> x0, other arithmetic: 5.88 us -> none  [block_grads(): causal = query_pos[:, None] >= key_pos[None, :]]
  transfers between devices with their start and end apart: 4 -> 2, of which waited for: 1 -> 2; matrix products, arithmetic and copies ran while one was open for 57% -> 2% of each run, Pallas kernels for 0% -> 0%
where the time goes in v1:
time: 147 us
  Pallas kernels  84.3 us (57%)
  waiting for transfers between devices  22.9 us (16%)
  between operations  14.3 us (10%)
  local copies, waits for them, and re-layouts  7.67 us (5%)
  other arithmetic  6.64 us (5%)
  starting transfers between devices  5.93 us (4%)
  matrix products  4.91 us (3%)
    pallas_call x1, Pallas kernels, attention(): pl.pallas_call(attention_kernel, out_shape=(jax.ShapeDtypeStruct((rows, 2...  84.3 us
    all_to_all x1, waiting for transfers between devices, summed_on_arrival(): lax.all_to_all(parts, axis, split_axis=0, concat_axis=0, tiled=True)  19.3 us
    all_to_all x1, starting transfers between devices, summed_on_arrival(): lax.all_to_all(parts, axis, split_axis=0, concat_axis=0, tiled=True)  5.9 us
    reduce_scatter x1, waiting for transfers between devices, per_device(): lax.psum_scatter(latent_partial.astype(jnp.bfloat16), 'tp', scatter_dimen...  3.55 us
    unnamed x27, local copies, waits for them, and re-layouts  3.1 us
  transfers between devices with their start and end apart: 2, of which 2 were waited for; matrix products, arithmetic and copies ran while one was open for 2% of the time, Pallas kernels for 0%

profile of v1, /device:TPU:8, one launch (start us, length us, event | category | flops | bytes accessed | tf_op | source)
XLA Modules:
  0.0 146.7 jit_solution(5669335725344397704)
XLA Ops:
  7.2 0.0 copy-start
  7.2 0.0 reduce-scatter.2.cloned.1.call-start
  7.2 0.7 multiply_bitcast_fusion
  8.0 0.7 broadcast_bitcast_fusion
  8.7 0.1 copy.22
  8.8 0.7 broadcast_multiply_fusion.1
  9.5 0.0 copy-start.8
  9.5 0.0 copy-start.9
  9.5 0.0 copy-start.4
  9.6 1.7 %convolution_convert_fusion.2 = bf16[288,256]{1,0:T(8,128)(2,1)S(1)} fusion(bf16[288,2048]{1,0:T(8,128)(2,1)S(1)} %copy-done, bf16[2048,256]{1,0:T(8,128)(2,1)} %param.12), kind=kOutput, calls=%fused_computation.4 | convolution fusion | flops 302063616 | bytes 2375680 | tf_op jit(solution)/shard_map/dot_general | solution.py:405
  11.3 0.0 copy-start.5
  11.3 0.0 copy-start.3
  11.3 0.0 copy-start.11
  11.4 0.0 copy-done.4
  11.4 0.1 reshape.42
  11.6 0.6 copy-done.5
  12.2 0.1 reshape.43
  12.4 0.1 reshape.44
  12.5 0.5 multiply_reduce_fusion.1
  13.1 0.7 multiply_reduce_fusion
  13.8 0.8 multiply_convert_fusion
  14.6 0.7 fusion.1
  15.3 0.1 copy.20
  15.4 0.1 copy.21
  15.5 0.1 stack.13.clone
  15.6 0.1 broadcast_subtract_fusion
  15.7 0.6 pad.10.sta_ref
  16.3 0.4 mul.79
  16.7 0.4 mul.88
  17.0 0.1 fusion.5
  17.2 0.4 dynamic_update_slice.3.stb_ref
  17.6 0.0 copy-start.10
  17.6 0.8 pad_maximum_fusion.1
  18.3 0.7 pad_maximum_fusion
  19.1 84.3 %shard_map.120 = (f32[288,256]{1,0:T(8,128)}, f32[288,256]{1,0:T(8,128)}, bf16[288,256]{1,0:T(8,128)(2,1)}) custom-call(bf16[288,256]{1,0:T(8,128)(2,1)} %get-tuple-element.24.ma_ref, bf16[288,256]{1,0:T(8,128)(2,1)} %get-tuple-element.26.na_ref, bf16[288,256]{1,0:T(8,128)(2,1)} %get-tuple-element.27.mb_ref, bf16[288,256]{1,0:T(8,128)(2,1)} %get-tuple-element.25.nb_ref, ...), custom_call_target="tpu_custom_call" | custom-call | flops 20000000000 | bytes 4000000 | tf_op jit(solution)/shard_map/pallas_call | solution.py:346
  103.5 2.4 %convolution_convert_fusion = bf16[288,2048]{1,0:T(8,128)(2,1)} fusion(bf16[288,256]{1,0:T(8,128)(2,1)} %get-tuple-element.9, bf16[2048,256]{1,0:T(8,128)(2,1)S(1)} %copy-done.1), kind=kOutput, calls=%fused_computation | convolution fusion | flops 302579712 | bytes 2375680 | tf_op jit(solution)/shard_map/dot_general | solution.py:428
  105.9 0.0 reduce-scatter.2.cloned.1.call-update
  105.9 0.9 copy-done.2
  106.8 0.7 fusion
  107.5 1.3 copy.19
  108.9 5.9 %all-to-all-start = ((bf16[32,64,256]{2,1,0:T(8,128)(2,1)}), bf16[32,64,256]{2,1,0:T(8,128)(2,1)S(1)}, u32[]{:S(2)}, u32[]{:S(2)}) async-start(bf16[32,64,256]{2,1,0:T(8,128)(2,1)} %bitcast.8), calls=%async_computation.1 | async-start | bytes 2097152 | tf_op jit(solution)/shard_map/all_to_all | solution.py:27
  114.8 19.3 %all-to-all-done = bf16[32,64,256]{2,1,0:T(8,128)(2,1)S(1)} async-done(((bf16[32,64,256]{2,1,0:T(8,128)(2,1)}), bf16[32,64,256]{2,1,0:T(8,128)(2,1)S(1)}, u32[]{:S(2)}, u32[]{:S(2)}) %all-to-all-start) | async-done | bytes 1048608 | tf_op jit(solution)/shard_map/all_to_all | solution.py:27
  134.1 0.8 convert_reduce_fusion
  134.9 3.6 %reduce-scatter.2.cloned.1.call-done = bf16[288,256]{1,0:T(8,128)(2,1)} async-done(((bf16[288,2048]{1,0:T(8,128)(2,1)}), bf16[288,256]{1,0:T(8,128)(2,1)}) %reduce-scatter.2.cloned.1.call-update) | async-done | bytes 147472 | tf_op jit(solution)/shard_map/reduce_scatter | solution.py:431
  138.4 0.0 copy-done.7
  138.4 0.7 copy.30
  139.1 0.0 copy-done.6
  139.1 0.7 copy.31
  (21 shorter events, 0.2 us)
Async XLA Ops:
  7.2 2.4 %copy-start = (bf16[288,2048]{1,0:T(8,128)(2,1)S(1)}, bf16[288,2048]{1,0:T(8,128)(2,1)}, u32[]{:S(2)}) copy-start(bf16[288,2048]{1,0:T(8,128)(2,1)} %param.11) | copy-start | bytes 3538948
  7.2 131.2 %reduce-scatter.2.cloned.1.call-start = ((), (), s32[]{:S(2)}) async-start(), calls=%async_computation.2 | async-start | bytes 1327104 | tf_op jit(solution)/shard_map/reduce_scatter | solution.py:431
  9.5 1.8 %copy-start.8 = (bf16[288,256]{1,0:T(8,128)(2,1)S(1)}, bf16[288,256]{1,0:T(8,128)(2,1)}, u32[]{:S(2)}) copy-start(bf16[288,256]{1,0:T(8,128)(2,1)} %param.9) | copy-start | bytes 442372
  9.5 1.9 %copy-start.9 = (bf16[288,256]{1,0:T(8,128)(2,1)S(1)}, bf16[288,256]{1,0:T(8,128)(2,1)}, u32[]{:S(2)}) copy-start(bf16[288,256]{1,0:T(8,128)(2,1)} %param.10) | copy-start | bytes 442372
  9.5 1.9 %copy-start.4 = (bf16[288,256]{1,0:T(8,128)(2,1)S(1)}, bf16[288,256]{1,0:T(8,128)(2,1)}, u32[]{:S(2)}) copy-start(bf16[288,256]{1,0:T(8,128)(2,1)} %param.14) | copy-start | bytes 442372
  11.3 0.9 copy-start.5
  11.3 1.1 copy-start.3
  11.3 1.2 copy-start.11
  17.6 1.5 %copy-start.10 = (f32[8,1152]{1,0:T(8,128)}, f32[8,1152]{1,0:T(8,128)S(1)}, u32[]{:S(2)}) copy-start(f32[8,1152]{1,0:T(8,128)S(1)} %dynamic_update_slice.3.stb_ref) | copy-start | bytes 110596
  19.1 84.4 %copy-start.1 = (bf16[2048,256]{1,0:T(8,128)(2,1)S(1)}, bf16[2048,256]{1,0:T(8,128)(2,1)}, u32[]{:S(2)}) copy-start(bf16[2048,256]{1,0:T(8,128)(2,1)} %param.12) | copy-start | bytes 3145732
  105.9 0.9 copy-start.2
  108.9 29.6 %copy-start.7 = (f32[288,256]{1,0:T(8,128)S(1)}, f32[288,256]{1,0:T(8,128)}, u32[]{:S(2)}) copy-start(f32[288,256]{1,0:T(8,128)} %get-tuple-element.32) | copy-start | bytes 884740
  108.9 25.2 %all-to-all-start = ((bf16[32,64,256]{2,1,0:T(8,128)(2,1)}), bf16[32,64,256]{2,1,0:T(8,128)(2,1)S(1)}, u32[]{:S(2)}, u32[]{:S(2)}) async-start(bf16[32,64,256]{2,1,0:T(8,128)(2,1)} %bitcast.8), calls=%async_computation.1 | async-start | bytes 2097152 | tf_op jit(solution)/shard_map/all_to_all | solution.py:27
  114.8 24.4 %copy-start.6 = (f32[288,256]{1,0:T(8,128)S(1)}, f32[288,256]{1,0:T(8,128)}, u32[]{:S(2)}) copy-start(f32[288,256]{1,0:T(8,128)} %get-tuple-element.33) | copy-start | bytes 884740
Sparse Core Ops, SparseCore 0:
  106.0 32.3 reduce-scatter.1

commit v2 on v1

v2 whole, which is shorter than its diff:
```python
import functools
import math

import jax
import jax.numpy as jnp
from jax import lax
from jax.experimental import pallas as pl
from jax.experimental.pallas import tpu as pltpu
from jax.sharding import PartitionSpec as P

DH = 64
DV = 128
NY = 4
NZ = 8
NX = 4
PIECES = 1
CHAIN = 4
LOG2E = math.log2(math.e)
BF = jnp.bfloat16
F32 = jnp.float32


def dot(a, b):
    return jnp.dot(a, b, preferred_element_type=F32)


def low_map(x):
    return lax.broadcasted_iota(jnp.int32, x.shape, 1) < DH


def score_terms(m_a, m_b, na_t, nb_t, shift0, shift1, dot0, dot1, mask):
    low = low_map(m_a)
    none = jnp.zeros_like(m_a)
    s0 = dot(jnp.where(low, m_a, none), na_t) * (LOG2E * DH ** (-0.5)) - shift0
    s1 = dot(jnp.where(low, none, m_a), na_t) * (LOG2E * DH ** (-0.5)) - shift1
    da = dot(m_b, nb_t)
    if mask is not None:
        s0 = jnp.where(mask, s0, -1e30)
        s1 = jnp.where(mask, s1, -1e30)
    p0 = jnp.exp2(s0)
    p1 = jnp.exp2(s1)
    ds0 = (p0 * (da - dot0)).astype(BF)
    ds1 = (p1 * (dot1 - da)).astype(BF)
    weights = (p0 - p1).astype(BF)
    return ds0, ds1, weights


def attention_kernel(
    q_ref, k_ref, lat_ref, wv_ref, lse_ref, first_ref, second_ref, cot_ref, lam_ref,
    gq_ref, gk_ref, gl_ref, gw_ref,
    ma, mb, sta, stb, stc, stw, na, nb, nat, nvt, nbt, ndt,
    acc_a, acc_v, acc_b, own_a, own_b, full_a, full_b,
    send_a, send_b, home_a, home_b, nsend_a, nsend_b, nrecv_a, nrecv_b,
    lperm, latg, gvg, dw_send, dw_recv, dl_send, dl_core, dl_pair, dl_recv,
    yg_send, yg_recv, ma_send, ma_recv, sta_send, sta_recv, mb_send, mb_recv,
    ra_send, rb_send, ha_recv, hb_recv,
    na_send, na_recv, nb_send, nb_recv,
    lat_send, lat_recv, gv_send, gv_recv, dw_ssem, dw_rsem, dc_send, dc_recv, dx_send, dx_recv,
):
    rows = q_ref.shape[0]
    wide = NY * rows
    sp = lax.axis_index("sp")
    tp = lax.axis_index("tp")
    z = sp // NY
    y = sp % NY
    x = tp // 2
    core = tp % 2

    def copy_to(src, dst, ssem, rsem, where):
        return pltpu.make_async_remote_copy(
            src_ref=src, dst_ref=dst, send_sem=ssem, recv_sem=rsem,
            device_id=where, device_id_type=pl.DeviceIdType.MESH,
        )

    def copy(src, dst, ssem, rsem, target):
        return copy_to(src, dst, ssem, rsem, {"sp": target})

    barrier = pltpu.get_barrier_semaphore()
    y_slots = [(y + k) % NY for k in range(1, NY)]
    z_slots = [(z + k) % NZ for k in range(1, NZ)]
    x_slots = [(x + k) % NX for k in range(1, NX)]
    y_peers = [z * NY + s for s in y_slots]
    z_peers = [s * NY + y for s in z_slots]
    other_core = {"tp": x * 2 + 1 - core}
    x_peers = [{"tp": s * 2 + core} for s in x_slots]
    everyone = [{"sp": p} for p in y_peers + z_peers] + [other_core] + x_peers
    for peer in everyone:
        pl.semaphore_signal(barrier, inc=1, device_id=peer, device_id_type=pl.DeviceIdType.MESH)

    def span(index):
        return pl.ds(pl.multiple_of(index * rows, rows), rows)

    last = NZ * NY - 1
    below = jnp.maximum(sp - NY, 0)
    above = jnp.minimum(sp + NY, last)
    lowest = y
    highest = (NZ - 1) * NY + y

    piece = rows // PIECES

    def ma_copies(src, st, c, target, far=0):
        return [copy(st, sta.at[c], sta_send.at[c, far], sta_recv.at[c], target)] + [
            copy(
                src.at[p * piece : (p + 1) * piece],
                ma.at[c, p * piece : (p + 1) * piece],
                ma_send.at[c, far * PIECES + p],
                ma_recv.at[c, p],
                target,
            )
            for p in range(PIECES)
        ]

    def mb_copies(src, c, target, far=0):
        return [
            copy(
                src.at[p * piece : (p + 1) * piece],
                mb.at[c, p * piece : (p + 1) * piece],
                mb_send.at[c, far * PIECES + p],
                mb_recv.at[c, p],
                target,
            )
            for p in range(PIECES)
        ]

    def y_copies(k, slot, target):
        return [
            lambda: copy(na.at[span(y)], na.at[span(slot)], yg_send.at[k, 0], yg_recv.at[slot, 0], target),
            lambda: copy(nb.at[span(y)], nb.at[span(slot)], yg_send.at[k, 1], yg_recv.at[slot, 1], target),
            lambda: copy(stb.at[y], stb.at[slot], yg_send.at[k, 2], yg_recv.at[slot, 2], target),
        ]

    def start(copies):
        for c in copies:
            c.start()

    values = dot(lat_ref[...], wv_ref[...]).astype(BF)
    k_own = k_ref[...]
    q_own = q_ref[...]
    which = lax.broadcasted_iota(jnp.int32, (rows, DV), 1)

    def row_terms(h):
        cols = slice(h * DV, (h + 1) * DV)
        first = first_ref[:, cols].astype(F32)
        second = second_ref[:, cols].astype(F32)
        grad_out = cot_ref[:, cols].astype(F32)
        lam = jnp.full((rows, 1), lam_ref[h], F32)
        mixed = first - lam * second
        inverse = lax.rsqrt(jnp.mean(mixed * mixed, axis=-1, keepdims=True) + 1e-06)
        normed = mixed * inverse
        mean = jnp.mean(grad_out * normed, axis=-1, keepdims=True)
        grad_rows = (inverse * (grad_out - normed * mean)).astype(BF)
        widened = grad_rows.astype(F32)
        dot0 = jnp.sum(widened * first, axis=-1, keepdims=True)
        dot1 = jnp.sum(widened * second, axis=-1, keepdims=True)
        stats = jnp.where(which < 3, dot0, dot1)
        stats = jnp.concatenate([stats, jnp.zeros((sta.shape[2] - rows, DV), F32)], axis=0)
        return grad_rows, stats.T[: sta.shape[1]]

    def shifts(h, m):
        shift = lse_ref[2 * h + m : 2 * h + m + 1, :] * LOG2E
        if m == 1:
            shift -= jnp.log(jnp.full((1, rows), lam_ref[h], F32)) * LOG2E
        return shift

    na[span(y), :DV] = k_own[:, :DV]
    na[span(y), DV:] = values[:, :DV]
    mb[z, :, :DV] = k_own[:, DV:]
    mb[z, :, DV:] = values[:, DV:]
    grad_rows, stats = row_terms(0)
    ma[z, :, :DV] = q_own[:, :DV]
    ma[z, :, DV:] = grad_rows
    sta[z] = stats
    sta[z, 0:1, :rows] = shifts(0, 0)
    sta[z, 1:2, :rows] = shifts(0, 1)
    grad_rows, stats = row_terms(1)
    nb[span(y), :DV] = q_own[:, DV:]
    nb[span(y), DV:] = grad_rows
    stb[y] = stats
    stb[y, 0:1, :rows] = shifts(1, 0)
    stb[y, 1:2, :rows] = shifts(1, 1)
    block = lat_ref.shape[1] // (NY * NZ)
    quarter = NZ * block
    for j in range(NY):
        for i in range(0, NZ, 2):
            one = (i * NY + j) * block
            two = (i * NY + NY + j) * block
            lperm[:, j * quarter + i * block : j * quarter + (i + 2) * block] = jnp.concatenate(
                [lat_ref[:, one : one + block], lat_ref[:, two : two + block]], axis=1
            )

    pl.semaphore_wait(barrier, len(everyone))

    @pl.when(z > 0)
    def _():
        start(ma_copies(ma.at[z], sta.at[z], z, below))

    @pl.when(z < NZ - 1)
    def _():
        start(mb_copies(mb.at[z], z, above))

    @pl.when(z > CHAIN)
    def _():
        start(ma_copies(ma.at[z], sta.at[z], z, lowest, 1))

    @pl.when(z < NZ - 1 - CHAIN)
    def _():
        start(mb_copies(mb.at[z], z, highest, 1))

    y_gather = [y_copies(k, y, peer) for k, peer in enumerate(y_peers)]
    for part in range(3):
        for k in range(NY - 1):
            y_gather[k][part]().start()

    def columns(index):
        return pl.ds(pl.multiple_of(index * quarter, quarter), quarter)

    def y_arrived(part):
        for k, peer in enumerate(y_peers):
            y_copies(k, y_slots[k], peer)[part]().wait_recv()

    def take_a(t):
        for c in ma_copies(ma.at[z + t], sta.at[z + t], z + t, below):
            c.wait_recv()

    def take_b(t):
        for c in mb_copies(mb.at[z - t], z - t, above):
            c.wait_recv()

    def pass_a(t):
        @pl.when(jnp.logical_and(jnp.logical_and(z > 0, t < CHAIN), z + t < NZ))
        def _():
            for c in ma_copies(ma.at[z + t], sta.at[z + t], z + t, below):
                c.wait_recv()
                c.start()

    def pass_b(t):
        @pl.when(jnp.logical_and(jnp.logical_and(z < NZ - 1, t < CHAIN), z - t >= 0))
        def _():
            for c in mb_copies(mb.at[z - t], z - t, above):
                c.wait_recv()
                c.start()

    def unit_a(m, stats, mask):
        st = stats.T[:rows]
        m_a = m[:, :DV]
        m_b = m[:, DV:]
        ds0, ds1, weights = score_terms(
            m_a, m_b, nat[...], nvt[...], st[:, 0:1], st[:, 1:2], st[:, 2:3], st[:, 3:4], mask
        )
        k_all = na[:, :DV]
        d0 = dot(ds0, k_all)
        d1 = dot(ds1, k_all)
        m_at = m_a.T
        parts = (dot(m_at[:DH], ds0), dot(m_at[DH:], ds1), dot(m_b.T, weights))
        return jnp.where(low_map(d0), d0, d1), parts

    def unit_b(m, mask):
        st = stw[...]
        m_a = m[:, :DV]
        m_b = m[:, DV:]
        ds0, ds1, weights = score_terms(
            m_a, m_b, nbt[...], ndt[...], st[0:1], st[1:2], st[2:3], st[3:4], mask
        )
        q_all = nb[:, :DV]
        d0 = dot(ds0, q_all)
        d1 = dot(ds1, q_all)
        dv = dot(weights, nb[:, DV:])
        m_at = m_a.T
        parts = (dot(m_at[:DH], ds0), dot(m_at[DH:], ds1))
        return jnp.where(low_map(d0), d0, d1), dv, parts

    lane = lax.broadcasted_iota(jnp.int32, (rows, wide), 1)
    place = lax.broadcasted_iota(jnp.int32, (rows, wide), 0) + y * rows

    def lat_copy(k, mine, theirs, target):
        return copy(lperm.at[:, columns(theirs)], latg.at[mine], lat_send.at[k], lat_recv.at[mine], target)

    latg[y] = lperm[:, columns(y)]
    acc_a[...] = jnp.zeros_like(acc_a)
    acc_v[...] = jnp.zeros_like(acc_v)
    acc_b[...] = jnp.zeros_like(acc_b)
    pass_a(1)
    pass_b(1)
    y_arrived(0)
    nat[...] = na[:, :DV].T
    nvt[...] = na[:, DV:].T

    def home_a_copy(t):
        return copy(
            send_a.at[t], home_a.at[t], ra_send.at[t], ha_recv.at[t], jnp.minimum(sp + t * NY, last)
        )

    def home_b_copy(t):
        return copy(
            send_b.at[t], home_b.at[t], rb_send.at[t], hb_recv.at[t], jnp.maximum(sp - t * NY, 0)
        )

    def chains_a(t):
        return jnp.logical_and(t < CHAIN, z > 0)

    def chains_b(t):
        return jnp.logical_and(t < CHAIN, z < NZ - 1)

    def step(n, carry):
        odd = n % 2
        t = odd * ((n + 1) // 2) + (1 - odd) * (NZ - n // 2)
        t = jnp.where(n < 2, 1 - n, t)
        all_seen = jnp.where(t == 0, 0, NY * rows)

        @pl.when(z + t < NZ)
        def _():
            @pl.when(jnp.logical_and(jnp.logical_not(chains_a(t)), t > 0))
            def _():
                take_a(t)

            @pl.when(t > CHAIN + 1)
            def _():
                start(ma_copies(ma.at[z + t], sta.at[z + t], z + t, above))

            moved, parts = unit_a(ma[z + t], sta[z + t], place + all_seen >= lane)
            acc_a[:DH] += parts[0]
            acc_a[DH:] += parts[1]
            acc_v[...] += parts[2]

            @pl.when(t > 0)
            def _():
                send_a[t] = moved.astype(BF)
                home_a_copy(t).start()

            @pl.when(t == 0)
            def _():
                own_a[...] = moved

        @pl.when(n < 2)
        def _():
            pass_a(n + 2)
            pass_b(n + 2)

        @pl.when(n == 0)
        def _():
            y_arrived(1)
            y_arrived(2)
            nbt[...] = nb[:, :DV].T
            ndt[...] = nb[:, DV:].T
            for j in range(NY):
                stc[j * rows : (j + 1) * rows, : stb.shape[1]] = stb[j].T[:rows]
            stw[...] = stc[...].T[: stw.shape[0]]
            for k, peer in enumerate(y_peers):
                lat_copy(k, y, y_slots[k], peer).start()

        @pl.when(z - t >= 0)
        def _():
            @pl.when(jnp.logical_and(jnp.logical_not(chains_b(t)), t > 0))
            def _():
                take_b(t)

            @pl.when(t > CHAIN + 1)
            def _():
                start(mb_copies(mb.at[z - t], z - t, below))

            moved, moved_v, parts = unit_b(mb[z - t], lane + all_seen >= place)
            acc_b[:DH] += parts[0]
            acc_b[DH:] += parts[1]

            @pl.when(t > 0)
            def _():
                send_b[t, :, :DV] = moved.astype(BF)
                send_b[t, :, DV:] = moved_v.astype(BF)
                home_b_copy(t).start()

            @pl.when(t == 0)
            def _():
                own_b[:, :DV] = moved
                own_b[:, DV:] = moved_v

        return carry

    lax.fori_loop(0, NZ, step, 0)

    def y_out_a(k, mine, theirs, target):
        return copy(nsend_a.at[span(theirs)], nrecv_a.at[mine], na_send.at[k], na_recv.at[mine], target)

    def y_out_b(k, mine, theirs, target):
        return copy(nsend_b.at[span(theirs)], nrecv_b.at[mine], nb_send.at[k], nb_recv.at[mine], target)

    full_a[:, :DV] = acc_a[...].T
    full_a[:, DV:] = acc_v[...].T
    nsend_a[...] = full_a[...].astype(BF)
    for k, peer in enumerate(y_peers):
        y_out_a(k, y, y_slots[k], peer).start()
    full_b[...] = acc_b[...].T
    nsend_b[...] = full_b[...].astype(BF)

    def home_a_wait(slot):
        copy(send_a.at[0], home_a.at[slot], ra_send.at[0], ha_recv.at[slot], below).wait_recv()
        own_a[...] += home_a[slot].astype(F32)

    def home_b_wait(slot):
        copy(send_b.at[0], home_b.at[slot], rb_send.at[0], hb_recv.at[slot], above).wait_recv()
        own_b[...] += home_b[slot].astype(F32)

    for slot in range(1, NZ):

        @pl.when(z + slot < NZ)
        def _(slot=slot):
            home_b_wait(slot)

    total_a = full_a[span(y), :]
    for k, peer in enumerate(y_peers):
        y_out_a(k, y_slots[k], y, peer).wait_recv()
        total_a += nrecv_a[y_slots[k]].astype(F32)
    gv = jnp.concatenate([total_a[:, DV:].astype(BF), own_b[:, DV:].astype(BF)], axis=1)
    gvg[y] = gv

    def gv_copy(k, mine, target):
        return copy(gvg.at[y], gvg.at[mine], gv_send.at[k], gv_recv.at[mine], target)

    for k, peer in enumerate(y_peers):
        gv_copy(k, y, peer).start()
    for k, peer in enumerate(y_peers):
        y_out_b(k, y, y_slots[k], peer).start()

    width = wv_ref.shape[0] // (2 * NX)

    def dl_part(tp_index):
        first = pl.multiple_of(tp_index * width, width)
        return lax.dot_general(
            gv, wv_ref[pl.ds(first, width), :], (((1,), (1,)), ((), ())), preferred_element_type=F32
        )

    def core_copy(j):
        return copy_to(dl_send.at[j], dl_core.at[j], dc_send.at[j], dc_recv.at[j], other_core)

    def x_copy(k, mine, theirs):
        return copy_to(dl_pair.at[theirs], dl_recv.at[mine], dx_send.at[k], dx_recv.at[mine], x_peers[k])

    for j in range(NX):
        dl_send[j] = dl_part(2 * j + 1 - core).astype(BF)
        core_copy(j).start()

    gk_ref[:, :DV] = total_a[:, :DV]
    gk_ref[:, DV:] = own_b[:, :DV]
    for k in range(NX):
        j = (x + k + 1) % NX
        mine = dl_part(2 * j + core)
        core_copy(j).wait_recv()
        dl_pair[j] = (mine + dl_core[j].astype(F32)).astype(BF)
        if k < NX - 1:
            x_copy(k, x, j).start()

    for k, peer in enumerate(y_peers):
        gv_copy(k, y_slots[k], peer).wait_recv()
        lat_copy(k, y_slots[k], y, peer).wait_recv()
    dw = dot(latg[0].T, gvg[0])
    for j in range(1, NY):
        dw += dot(latg[j].T, gvg[j])
    for j in range(NZ):
        dw_send[j] = dw[j * block : (j + 1) * block].astype(BF)

    def dw_copy(k, mine, theirs, target):
        return copy(dw_send.at[theirs], dw_recv.at[mine], dw_ssem.at[k], dw_rsem.at[mine], target)

    for k, peer in enumerate(z_peers):
        dw_copy(k, z, z_slots[k], peer).start()

    for slot in range(1, NZ):

        @pl.when(z - slot >= 0)
        def _(slot=slot):
            home_a_wait(slot)

    total_b = full_b[span(y), :]
    for k, peer in enumerate(y_peers):
        y_out_b(k, y_slots[k], y, peer).wait_recv()
        total_b += nrecv_b[y_slots[k]].astype(F32)
    gq_ref[:, :DV] = own_a[...]
    gq_ref[:, DV:] = total_b

    gl = dl_pair[x].astype(F32)
    for k in range(NX - 1):
        x_copy(k, x_slots[k], x).wait_recv()
        gl += dl_recv[x_slots[k]].astype(F32)
    gl_ref[...] = gl.astype(BF)

    gw = dw_send[z].astype(F32)
    for k, peer in enumerate(z_peers):
        dw_copy(k, z_slots[k], z, peer).wait_recv()
        gw += dw_recv[z_slots[k]].astype(F32)
    gw_ref[...] = gw

    for k, peer in enumerate(y_peers):
        for c in y_copies(k, y, peer):
            c().wait_send()
        lat_copy(k, y, y_slots[k], peer).wait_send()
        gv_copy(k, y, peer).wait_send()
        y_out_a(k, y, y, peer).wait_send()
        y_out_b(k, y, y, peer).wait_send()
    for k, peer in enumerate(z_peers):
        dw_copy(k, z, z_slots[k], peer).wait_send()
    for j in range(NX):
        core_copy(j).wait_send()
    for k in range(NX - 1):
        x_copy(k, x, x_slots[k]).wait_send()

    def sent(copies):
        for c in copies:
            c.wait_send()

    @pl.when(z > CHAIN)
    def _():
        sent(ma_copies(ma.at[z], sta.at[z], z, lowest, 1))

    @pl.when(z < NZ - 1 - CHAIN)
    def _():
        sent(mb_copies(mb.at[z], z, highest, 1))

    def drain_a(t, carry):
        @pl.when(t > 0)
        def _():
            home_a_copy(t).wait_send()

        @pl.when(jnp.logical_or(chains_a(t), t > CHAIN + 1))
        def _():
            sent(ma_copies(ma.at[z + t], sta.at[z + t], z + t, below))

        return carry

    def drain_b(t, carry):
        @pl.when(t > 0)
        def _():
            home_b_copy(t).wait_send()

        @pl.when(jnp.logical_or(chains_b(t), t > CHAIN + 1))
        def _():
            sent(mb_copies(mb.at[z - t], z - t, above))

        return carry

    lax.fori_loop(0, NZ - z, drain_a, 0)
    lax.fori_loop(0, z + 1, drain_b, 0)


def attention(queries, key_vectors, latents, value_weight, log_sums, out_first, out_second, cotangent, head_lambda):
    rows = queries.shape[0]
    wide = NY * rows
    depth = latents.shape[1]
    piece = depth // (NY * NZ)
    part = depth // (2 * NX)
    dma = pltpu.SemaphoreType.DMA
    vmem = pltpu.VMEM
    whole = pl.BlockSpec(memory_space=pltpu.VMEM)
    both = (rows, 2 * DV)
    stats = (8, rows + -rows % 128)
    return pl.pallas_call(
        attention_kernel,
        out_shape=(
            jax.ShapeDtypeStruct(both, F32),
            jax.ShapeDtypeStruct(both, F32),
            jax.ShapeDtypeStruct((rows, part), BF),
            jax.ShapeDtypeStruct((piece, 2 * DV), F32),
        ),
        in_specs=[whole] * 8 + [pl.BlockSpec(memory_space=pltpu.SMEM)],
        out_specs=(whole,) * 4,
        scratch_shapes=[
            vmem((NZ,) + both, BF),
            vmem((NZ,) + both, BF),
            vmem((NZ,) + stats, F32),
            vmem((NY,) + stats, F32),
            vmem((wide, DV), F32),
            vmem((stats[0], wide), F32),
            vmem((wide, 2 * DV), BF),
            vmem((wide, 2 * DV), BF),
            vmem((DV, wide), BF),
            vmem((DV, wide), BF),
            vmem((DV, wide), BF),
            vmem((DV, wide), BF),
            vmem((DV, wide), F32),
            vmem((DV, wide), F32),
            vmem((DV, wide), F32),
            vmem((rows, DV), F32),
            vmem(both, F32),
            vmem((wide, 2 * DV), F32),
            vmem((wide, DV), F32),
            vmem((NZ, rows, DV), BF),
            vmem((NZ,) + both, BF),
            vmem((NZ, rows, DV), BF),
            vmem((NZ,) + both, BF),
            vmem((wide, 2 * DV), BF),
            vmem((wide, DV), BF),
            vmem((NY,) + both, BF),
            vmem((NY, rows, DV), BF),
            vmem((rows, depth), BF),
            vmem((NY, rows, NZ * piece), BF),
            vmem((NY,) + both, BF),
            vmem((NZ, piece, 2 * DV), BF),
            vmem((NZ, piece, 2 * DV), BF),
            vmem((NX, rows, part), BF),
            vmem((NX, rows, part), BF),
            vmem((NX, rows, part), BF),
            vmem((NX, rows, part), BF),
            dma((NY - 1, 3)),
            dma((NY, 3)),
        ]
        + [dma((NZ, 2 * PIECES)), dma((NZ, PIECES)), dma((NZ, 2)), dma((NZ,))]
        + [dma((NZ, 2 * PIECES)), dma((NZ, PIECES))]
        + [dma((NZ,))] * 4
        + [dma((NY,))] * 8
        + [dma((NZ,))] * 2
        + [dma((NX,))] * 4,
        compiler_params=pltpu.CompilerParams(
            collective_id=0, has_side_effects=True, vmem_limit_bytes=60 * 1024 * 1024
        ),
        cost_estimate=pl.CostEstimate(flops=20_000_000_000, bytes_accessed=4_000_000, transcendentals=6_000_000),
    )(queries, key_vectors, latents, value_weight, log_sums, out_first, out_second, cotangent, head_lambda)


def per_device(
    queries,
    key_vectors,
    latents,
    value_weight,
    log_sums,
    out_first,
    out_second,
    cotangent,
    head_lambda,
):
    grad_queries, grad_keys, grad_latents, grad_weight = attention(
        queries, key_vectors, latents, value_weight, log_sums.T, out_first, out_second, cotangent, head_lambda
    )
    scale = DH ** (-0.5)
    grad_queries, grad_keys = grad_queries * scale, grad_keys * scale
    return (grad_queries, grad_keys, grad_latents, grad_weight)


def solution(mesh):
    return jax.shard_map(
        per_device,
        mesh=mesh,
        in_specs=(
            P("sp", "tp"),
            P("sp", "tp"),
            P("sp", None),
            P(None, "tp"),
            P("sp", "tp"),
            P("sp", "tp"),
            P("sp", "tp"),
            P("sp", "tp"),
            P("tp"),
        ),
        out_specs=(P("sp", "tp"), P("sp", "tp"), P("sp", "tp"), P("sp", "tp")),
        check_vma=False,
    )
```

time: 147 us -> 84.3 us (0.57)
  the two profiles are of different devices: /device:TPU:8 before, /device:TPU:5 now
where the time goes in v2:
time: 84.3 us; the launch traced here: 84.1 us
  Pallas kernels  80.2 us (95%)
  other arithmetic  1.94 us (2%)
  local copies, waits for them, and re-layouts  1.3 us (2%)
    pallas_call x1, Pallas kernels, attention(): pl.pallas_call(attention_kernel, out_shape=(jax.ShapeDtypeStruct(both, F3...  80.2 us
    mul x1, other arithmetic, per_device(): grad_queries, grad_keys = (grad_queries * scale, grad_keys * scale)  1.94 us

profile of v2, /device:TPU:5, one launch (start us, length us, event | category | flops | bytes accessed | tf_op | source)
XLA Modules:
  0.0 84.1 jit_solution(6822537746017720105)
XLA Ops:
  0.6 80.2 %shard_map.120 = (f32[288,256]{1,0:T(8,128)}, f32[288,256]{1,0:T(8,128)}, bf16[288,256]{1,0:T(8,128)(2,1)}, f32[64,256]{1,0:T(8,128)}) custom-call(bf16[288,256]{1,0:T(8,128)(2,1)} %q_ref.1, bf16[288,256]{1,0:T(8,128)(2,1)} %k_ref.1, bf16[288,2048]{1,0:T(8,128)(2,1)} %lat_ref.1, bf16[2048,256]{1,0:T(8,128)(2,1)} %wv_ref.1, f32[4,288]{1,0:T(4,128)} %bitcast.1, ...), custom_call_target="tpu_custom_call" | custom-call | flops 20000000000 | bytes 4000000 | tf_op jit(solution)/shard_map/pallas_call | solution.py:554
  80.9 0.0 copy-start
  80.9 0.0 copy-start.1
  80.9 1.9 %broadcast_multiply_fusion = (f32[288,256]{1,0:T(8,128)}, f32[288,256]{1,0:T(8,128)}) fusion(f32[288,256]{1,0:T(8,128)} %get-tuple-element.9, f32[288,256]{1,0:T(8,128)} %get-tuple-element.8), kind=kLoop, calls=%fused_computation | loop fusion | flops 147456 | bytes 1179648 | tf_op jit(solution)/shard_map/mul | solution.py:632
  82.8 0.0 copy-done
  82.8 0.7 copy.15
  83.5 0.0 copy-done.1
  83.5 0.6 copy.16
Async XLA Ops:
  80.9 2.0 %copy-start = (bf16[288,256]{1,0:T(8,128)(2,1)S(1)}, bf16[288,256]{1,0:T(8,128)(2,1)}, u32[]{:S(2)}) copy-start(bf16[288,256]{1,0:T(8,128)(2,1)} %get-tuple-element.20) | copy-start | bytes 442372
  80.9 2.6 %copy-start.1 = (f32[64,256]{1,0:T(8,128)S(1)}, f32[64,256]{1,0:T(8,128)}, u32[]{:S(2)}) copy-start(f32[64,256]{1,0:T(8,128)} %get-tuple-element.21) | copy-start | bytes 196612

commit v3 on v2

--- a/solution.py
+++ b/solution.py
@@ -14,6 +14,7 @@
 NZ = 8
 NX = 4
 PIECES = 1
+HOME = (1, 3, 5, 6, 7)
 CHAIN = 4
 LOG2E = math.log2(math.e)
 BF = jnp.bfloat16
@@ -50,10 +51,10 @@
     gq_ref, gk_ref, gl_ref, gw_ref,
     ma, mb, sta, stb, stc, stw, na, nb, nat, nvt, nbt, ndt,
     acc_a, acc_v, acc_b, own_a, own_b, full_a, full_b,
-    send_a, send_b, home_a, home_b, nsend_a, nsend_b, nrecv_a, nrecv_b,
+    send_a, send_b, home_a, home_b, pair_a, pair_b, nsend_a, nsend_b, nrecv_a, nrecv_b,
     lperm, latg, gvg, dw_send, dw_recv, dl_send, dl_core, dl_pair, dl_recv,
     yg_send, yg_recv, ma_send, ma_recv, sta_send, sta_recv, mb_send, mb_recv,
-    ra_send, rb_send, ha_recv, hb_recv,
+    ra_send, rb_send, ha_recv, hb_recv, rk_send, hk_recv, pa_recv, pb_recv,
     na_send, na_recv, nb_send, nb_recv,
     lat_send, lat_recv, gv_send, gv_recv, dw_ssem, dw_rsem, dc_send, dc_recv, dx_send, dx_recv,
 ):
@@ -290,10 +291,18 @@
             send_a.at[t], home_a.at[t], ra_send.at[t], ha_recv.at[t], jnp.minimum(sp + t * NY, last)
         )
 
-    def home_b_copy(t):
-        return copy(
-            send_b.at[t], home_b.at[t], rb_send.at[t], hb_recv.at[t], jnp.maximum(sp - t * NY, 0)
-        )
+    def home_b_copies(t):
+        target = jnp.maximum(sp - t * NY, 0)
+        return [
+            copy(send_b.at[t, :, DV:], home_b.at[t, :, DV:], rb_send.at[t], hb_recv.at[t], target),
+            copy(send_b.at[t, :, :DV], home_b.at[t, :, :DV], rk_send.at[t], hk_recv.at[t], target),
+        ]
+
+    def pair_a_copy(t):
+        return copy(send_a.at[t], pair_a.at[t], ra_send.at[t], pa_recv.at[t], above)
+
+    def pair_b_copy(t):
+        return copy(send_b.at[t], pair_b.at[t], rb_send.at[t], pb_recv.at[t], below)
 
     def chains_a(t):
         return jnp.logical_and(t < CHAIN, z > 0)
@@ -303,8 +312,15 @@
 
     def step(n, carry):
         odd = n % 2
-        t = odd * ((n + 1) // 2) + (1 - odd) * (NZ - n // 2)
-        t = jnp.where(n < 2, 1 - n, t)
+        t = (1 - odd) * (NZ - n // 2)
+        t = jnp.where(n == 0, 0, t)
+        t = jnp.where(n == 1, 2, t)
+        t = jnp.where(n == 3, 1, t)
+        t = jnp.where(n == 5, 4, t)
+        t = jnp.where(n == 7, 3, t)
+        meets = jnp.logical_or(t == 1, t == 3)
+        joins = jnp.logical_or(t == 2, t == 4)
+        home = jnp.logical_and(t > 0, jnp.logical_not(joins))
         all_seen = jnp.where(t == 0, 0, NY * rows)
 
         @pl.when(z + t < NZ)
@@ -322,9 +338,21 @@
             acc_a[DH:] += parts[1]
             acc_v[...] += parts[2]
 
-            @pl.when(t > 0)
+            @pl.when(jnp.logical_and(meets, z > 0))
+            def _():
+                pair_a_copy(t + 1).wait_recv()
+                send_a[t] = (moved + pair_a[t + 1].astype(F32)).astype(BF)
+
+            @pl.when(jnp.logical_not(jnp.logical_and(meets, z > 0)))
             def _():
                 send_a[t] = moved.astype(BF)
+
+            @pl.when(joins)
+            def _():
+                pair_a_copy(t).start()
+
+            @pl.when(home)
+            def _():
                 home_a_copy(t).start()
 
             @pl.when(t == 0)
@@ -362,11 +390,24 @@
             acc_b[:DH] += parts[0]
             acc_b[DH:] += parts[1]
 
-            @pl.when(t > 0)
+            @pl.when(jnp.logical_and(meets, z < NZ - 1))
+            def _():
+                pair_b_copy(t + 1).wait_recv()
+                send_b[t, :, :DV] = (moved + pair_b[t + 1, :, :DV].astype(F32)).astype(BF)
+                send_b[t, :, DV:] = (moved_v + pair_b[t + 1, :, DV:].astype(F32)).astype(BF)
+
+            @pl.when(jnp.logical_not(jnp.logical_and(meets, z < NZ - 1)))
             def _():
                 send_b[t, :, :DV] = moved.astype(BF)
                 send_b[t, :, DV:] = moved_v.astype(BF)
-                home_b_copy(t).start()
+
+            @pl.when(joins)
+            def _():
+                pair_b_copy(t).start()
+
+            @pl.when(home)
+            def _():
+                home_b_copies(t)[0].start()
 
             @pl.when(t == 0)
             def _():
@@ -390,35 +431,67 @@
         y_out_a(k, y, y_slots[k], peer).start()
     full_b[...] = acc_b[...].T
     nsend_b[...] = full_b[...].astype(BF)
+    for k, peer in enumerate(y_peers):
+        y_out_b(k, y, y_slots[k], peer).start()
+    for t in HOME:
+
+        @pl.when(z - t >= 0)
+        def _(t=t):
+            home_b_copies(t)[1].start()
 
     def home_a_wait(slot):
         copy(send_a.at[0], home_a.at[slot], ra_send.at[0], ha_recv.at[slot], below).wait_recv()
         own_a[...] += home_a[slot].astype(F32)
 
-    def home_b_wait(slot):
-        copy(send_b.at[0], home_b.at[slot], rb_send.at[0], hb_recv.at[slot], above).wait_recv()
-        own_b[...] += home_b[slot].astype(F32)
-
-    for slot in range(1, NZ):
-
-        @pl.when(z + slot < NZ)
-        def _(slot=slot):
-            home_b_wait(slot)
+    def home_b_wait(slot, part):
+        sems = (hb_recv, hk_recv)[part]
+        cols = (slice(DV, 2 * DV), slice(0, DV))[part]
+        copy(
+            send_b.at[0, :, cols], home_b.at[slot, :, cols], rb_send.at[0], sems.at[slot], above
+        ).wait_recv()
+        own_b[:, cols] += home_b[slot, :, cols].astype(F32)
+
+    def gv_copy(k, mine, target, h):
+        cols = slice(h * DV, (h + 1) * DV)
+        return copy(
+            gvg.at[y, :, cols], gvg.at[mine, :, cols], gv_send.at[k, h], gv_recv.at[mine, h], target
+        )
+
+    def dw_copy(k, mine, theirs, target, h):
+        cols = slice(h * DV, (h + 1) * DV)
+        return copy(
+            dw_send.at[theirs, :, cols], dw_recv.at[mine, :, cols], dw_ssem.at[k, h], dw_rsem.at[mine, h], target
+        )
+
+    def weight_part(h):
+        for k, peer in enumerate(y_peers):
+            gv_copy(k, y_slots[k], peer, h).wait_recv()
+        cols = slice(h * DV, (h + 1) * DV)
+        dw = dot(latg[0].T, gvg[0, :, cols])
+        for j in range(1, NY):
+            dw += dot(latg[j].T, gvg[j, :, cols])
+        for j in range(NZ):
+            dw_send[j, :, cols] = dw[j * block : (j + 1) * block].astype(BF)
+        for k, peer in enumerate(z_peers):
+            dw_copy(k, z, z_slots[k], peer, h).start()
 
     total_a = full_a[span(y), :]
     for k, peer in enumerate(y_peers):
         y_out_a(k, y_slots[k], y, peer).wait_recv()
         total_a += nrecv_a[y_slots[k]].astype(F32)
-    gv = jnp.concatenate([total_a[:, DV:].astype(BF), own_b[:, DV:].astype(BF)], axis=1)
-    gvg[y] = gv
-
-    def gv_copy(k, mine, target):
-        return copy(gvg.at[y], gvg.at[mine], gv_send.at[k], gv_recv.at[mine], target)
-
+    gvg[y, :, :DV] = total_a[:, DV:].astype(BF)
     for k, peer in enumerate(y_peers):
-        gv_copy(k, y, peer).start()
+        gv_copy(k, y, peer, 0).start()
+    for slot in HOME:
+
+        @pl.when(z + slot < NZ)
+        def _(slot=slot):
+            home_b_wait(slot, 0)
+
+    gvg[y, :, DV:] = own_b[:, DV:].astype(BF)
     for k, peer in enumerate(y_peers):
-        y_out_b(k, y, y_slots[k], peer).start()
+        gv_copy(k, y, peer, 1).start()
+    gv = gvg[y]
 
     width = wv_ref.shape[0] // (2 * NX)
 
@@ -438,8 +511,6 @@
         dl_send[j] = dl_part(2 * j + 1 - core).astype(BF)
         core_copy(j).start()
 
-    gk_ref[:, :DV] = total_a[:, :DV]
-    gk_ref[:, DV:] = own_b[:, :DV]
     for k in range(NX):
         j = (x + k + 1) % NX
         mine = dl_part(2 * j + core)
@@ -449,26 +520,22 @@
             x_copy(k, x, j).start()
 
     for k, peer in enumerate(y_peers):
-        gv_copy(k, y_slots[k], peer).wait_recv()
         lat_copy(k, y_slots[k], y, peer).wait_recv()
-    dw = dot(latg[0].T, gvg[0])
-    for j in range(1, NY):
-        dw += dot(latg[j].T, gvg[j])
-    for j in range(NZ):
-        dw_send[j] = dw[j * block : (j + 1) * block].astype(BF)
-
-    def dw_copy(k, mine, theirs, target):
-        return copy(dw_send.at[theirs], dw_recv.at[mine], dw_ssem.at[k], dw_rsem.at[mine], target)
-
-    for k, peer in enumerate(z_peers):
-        dw_copy(k, z, z_slots[k], peer).start()
-
-    for slot in range(1, NZ):
+    weight_part(0)
+    weight_part(1)
+
+    for slot in HOME:
 
         @pl.when(z - slot >= 0)
         def _(slot=slot):
             home_a_wait(slot)
 
+        @pl.when(z + slot < NZ)
+        def _(slot=slot):
+            home_b_wait(slot, 1)
+
+    gk_ref[:, :DV] = total_a[:, :DV]
+    gk_ref[:, DV:] = own_b[:, :DV]
     total_b = full_b[span(y), :]
     for k, peer in enumerate(y_peers):
         y_out_b(k, y_slots[k], y, peer).wait_recv()
@@ -484,7 +551,8 @@
 
     gw = dw_send[z].astype(F32)
     for k, peer in enumerate(z_peers):
-        dw_copy(k, z_slots[k], z, peer).wait_recv()
+        dw_copy(k, z_slots[k], z, peer, 0).wait_recv()
+        dw_copy(k, z_slots[k], z, peer, 1).wait_recv()
         gw += dw_recv[z_slots[k]].astype(F32)
     gw_ref[...] = gw
 
@@ -492,11 +560,13 @@
         for c in y_copies(k, y, peer):
             c().wait_send()
         lat_copy(k, y, y_slots[k], peer).wait_send()
-        gv_copy(k, y, peer).wait_send()
+        gv_copy(k, y, peer, 0).wait_send()
+        gv_copy(k, y, peer, 1).wait_send()
         y_out_a(k, y, y, peer).wait_send()
         y_out_b(k, y, y, peer).wait_send()
     for k, peer in enumerate(z_peers):
-        dw_copy(k, z, z_slots[k], peer).wait_send()
+        dw_copy(k, z, z_slots[k], peer, 0).wait_send()
+        dw_copy(k, z, z_slots[k], peer, 1).wait_send()
     for j in range(NX):
         core_copy(j).wait_send()
     for k in range(NX - 1):
@@ -526,9 +596,15 @@
         return carry
 
     def drain_b(t, carry):
-        @pl.when(t > 0)
-        def _():
-            home_b_copy(t).wait_send()
+        joins = jnp.logical_or(t == 2, t == 4)
+
+        @pl.when(joins)
+        def _():
+            pair_b_copy(t).wait_send()
+
+        @pl.when(jnp.logical_and(t > 0, jnp.logical_not(joins)))
+        def _():
+            sent(home_b_copies(t))
 
         @pl.when(jnp.logical_or(chains_b(t), t > CHAIN + 1))
         def _():
@@ -585,6 +661,8 @@
             vmem((NZ,) + both, BF),
             vmem((NZ, rows, DV), BF),
             vmem((NZ,) + both, BF),
+            vmem((CHAIN + 1, rows, DV), BF),
+            vmem((CHAIN + 1,) + both, BF),
             vmem((wide, 2 * DV), BF),
             vmem((wide, DV), BF),
             vmem((NY,) + both, BF),
@@ -603,9 +681,11 @@
         ]
         + [dma((NZ, 2 * PIECES)), dma((NZ, PIECES)), dma((NZ, 2)), dma((NZ,))]
         + [dma((NZ, 2 * PIECES)), dma((NZ, PIECES))]
-        + [dma((NZ,))] * 4
-        + [dma((NY,))] * 8
-        + [dma((NZ,))] * 2
+        + [dma((NZ,))] * 6
+        + [dma((CHAIN + 1,))] * 2
+        + [dma((NY,))] * 6
+        + [dma((NY, 2))] * 2
+        + [dma((NZ, 2))] * 2
         + [dma((NX,))] * 4,
         compiler_params=pltpu.CompilerParams(
             collective_id=0, has_side_effects=True, vmem_limit_bytes=60 * 1024 * 1024

time: 84.3 us -> 80.3 us (0.953)
  the two profiles are of different devices: /device:TPU:5 before, /device:TPU:33 now
where the time goes in v3:
time: 80.3 us; the launch traced here: 80.1 us
  Pallas kernels  76.2 us (95%)
  other arithmetic  1.94 us (2%)
  local copies, waits for them, and re-layouts  1.3 us (2%)
    pallas_call x1, Pallas kernels, attention(): pl.pallas_call(attention_kernel, out_shape=(jax.ShapeDtypeStruct(both, F3...  76.2 us
    mul x1, other arithmetic, per_device(): grad_queries, grad_keys = (grad_queries * scale, grad_keys * scale)  1.94 us

profile of v3, /device:TPU:33, one launch (start us, length us, event | category | flops | bytes accessed | tf_op | source)
XLA Modules:
  0.0 80.1 jit_solution(8409233577420583655)
XLA Ops:
  0.6 76.2 %shard_map.120 = (f32[288,256]{1,0:T(8,128)}, f32[288,256]{1,0:T(8,128)}, bf16[288,256]{1,0:T(8,128)(2,1)}, f32[64,256]{1,0:T(8,128)}) custom-call(bf16[288,256]{1,0:T(8,128)(2,1)} %q_ref.1, bf16[288,256]{1,0:T(8,128)(2,1)} %k_ref.1, bf16[288,2048]{1,0:T(8,128)(2,1)} %lat_ref.1, bf16[2048,256]{1,0:T(8,128)(2,1)} %wv_ref.1, f32[4,288]{1,0:T(4,128)} %bitcast.1, ...), custom_call_target="tpu_custom_call" | custom-call | flops 20000000000 | bytes 4000000 | tf_op jit(solution)/shard_map/pallas_call | solution.py:630
  76.9 0.0 copy-start
  76.9 0.0 copy-start.1
  76.9 1.9 %broadcast_multiply_fusion = (f32[288,256]{1,0:T(8,128)}, f32[288,256]{1,0:T(8,128)}) fusion(f32[288,256]{1,0:T(8,128)} %get-tuple-element.9, f32[288,256]{1,0:T(8,128)} %get-tuple-element.8), kind=kLoop, calls=%fused_computation | loop fusion | flops 147456 | bytes 1179648 | tf_op jit(solution)/shard_map/mul | solution.py:712
  78.8 0.0 copy-done
  78.9 0.7 copy.15
  79.5 0.0 copy-done.1
  79.5 0.6 copy.16
Async XLA Ops:
  76.9 2.0 %copy-start = (bf16[288,256]{1,0:T(8,128)(2,1)S(1)}, bf16[288,256]{1,0:T(8,128)(2,1)}, u32[]{:S(2)}) copy-start(bf16[288,256]{1,0:T(8,128)(2,1)} %get-tuple-element.20) | copy-start | bytes 442372
  76.9 2.6 %copy-start.1 = (f32[64,256]{1,0:T(8,128)S(1)}, f32[64,256]{1,0:T(8,128)}, u32[]{:S(2)}) copy-start(f32[64,256]{1,0:T(8,128)} %get-tuple-element.21) | copy-start | bytes 196612
